TPU v7x, 512 devices: a whole 4x4x16 slice. The times are simulated.
512 devices in a mesh: sp: 32 (over z, core), tp: 16 (over y, x).
Axes of the slice: x: 4, y: 4, z: 16, core: 2. Of those that a mesh axis runs over, the one named last changes fastest.
Arguments:
- query_rows: bfloat16 [8192, 2048], P('sp', 'tp'), may hold values from -1000 to 1000
- key_rows: bfloat16 [8192, 256], P('sp'), may hold values from -6 to 6
- value_rows: bfloat16 [8192, 256], P('sp'), may hold values from -6 to 6
- sink_logits: float32 [32], P('tp'), may hold values from 1 to 6
- out_weight: bfloat16 [2048, 2048], P('tp'), may hold values from -0.375 to 0.375
- stream_in: bfloat16 [8192, 2048], P('sp'), may hold values from -6 to 6
- norm_gain: float32 [2048], replicated, may hold values from 0.1 to 1.9
- routes: int32 [8192, 2], P('sp'), may hold values from 0 to 31, all different within a row; in each aligned block of 256 rows (0 to 255, 256 to 511, ...) at most 24 rows name the same one
- route_weights: float32 [8192, 2], P('sp'), may hold values from 0.2 to 1
- gate_weight: bfloat16 [32, 2048, 4096], P('sp', None, 'tp'), may hold values from -0.125 to 0.125
- up_weight: bfloat16 [32, 2048, 4096], P('sp', None, 'tp'), may hold values from -0.125 to 0.125
- down_weight: bfloat16 [32, 4096, 2048], P('sp', 'tp'), may hold values from -0.09375 to 0.09375
Outputs:
- layer_out: bfloat16 [8192, 2048], P(('sp', 'tp'))
Inputs may be any that keep to these rules, and one draw needn't show every extreme that they name: `routes`: each row names 2 different experts. Within the rows of one device (256 aligned rows) no expert is named more than 24 times, a bound that some block reaches.
All inputs are finite; a program needn't handle non-finite values.
Results may differ from a plain program's by a relative error of at most 0.015.
Values may be sent and summed in bfloat16 or wider, within the bound.
No kernel may reach another device: no remote copies, remote signals or barrier semaphores. Data moves between devices by JAX's collectives and lax.ppermute only.
A program may use at most 64 MiB of HBM per device.

v0:
```python
import jax
import jax.numpy as jnp
from jax import lax
from jax.sharding import Mesh
from jax.sharding import PartitionSpec as P

HEAD_DIM = 64
REP = 8
WINDOW = 128
TP = ("tp_0", "tp_1")
SP_TP = ("sp", "tp_0", "tp_1")
norm_eps = 1e-06


def shifted(block, axis, distance):
    devices = range(lax.axis_size(axis))
    route = [(i - distance, i) for i in devices if i - distance in devices]
    return lax.ppermute(block, axis, route)


def cut_along(shard, dim, count):
    before, after = (shard.shape[:dim], shard.shape[dim + 1 :])
    return jnp.moveaxis(shard.reshape(*before, count, -1, *after), dim, 0)


def sum_at_owner(shard, axis, dim):
    pieces = cut_along(shard, dim, lax.axis_size(axis))
    arrived = lax.all_to_all(pieces, axis, split_axis=0, concat_axis=0, tiled=True)
    return arrived.astype(jnp.float32).sum(axis=0)


def laid_out(pieces, dim):
    lengths = list(pieces.shape[1:])
    lengths[dim] *= pieces.shape[0]
    return jnp.moveaxis(pieces, 0, dim).reshape(lengths)


def sent_to_all(shard, axis):
    copies = jnp.broadcast_to(shard, (lax.axis_size(axis), *shard.shape))
    return lax.all_to_all(copies, axis, split_axis=0, concat_axis=0, tiled=True)


def gathered_copies(shard, axis, dim):
    return laid_out(sent_to_all(shard, axis), dim)


def gathered_by_axis(shard, axes, dim):
    result = shard
    for number in range(len(axes) - 1, -1, -1):
        result = lax.all_gather(result, axes[number], axis=dim, tiled=True)
    return result


def piece_ends(length, count):
    hop = length // count
    if hop >= 8:
        hop -= hop % 8
    return [hop * k for k in range(1, count)]


def exchange_in_pieces(shard, axis, pieces, split_dim, concat_dim):
    blocks = cut_along(shard, split_dim, lax.axis_size(axis))
    split_at = max(range(1, max(2, blocks.ndim - 1)), key=lambda d: blocks.shape[d])
    finished = []
    for slab in jnp.split(blocks, piece_ends(blocks.shape[split_at], pieces), axis=split_at):
        if slab.size:
            finished.append(lax.all_to_all(slab, axis, split_axis=0, concat_axis=0, tiled=True))
    return laid_out(jnp.concatenate(finished, axis=split_at), concat_dim)


def rms_scale(stream, norm_gain):
    values = stream.astype(jnp.float32)
    scaled = values * lax.rsqrt(jnp.mean(values * values, axis=-1, keepdims=True) + norm_eps)
    return (scaled * norm_gain).astype(jnp.bfloat16)


def slot_tables(routes, experts_n, slot_cap):
    flat_ids = routes.reshape(-1)
    onehot = (flat_ids[:, None] == jnp.arange(experts_n, dtype=jnp.int32)[None, :]).astype(
        jnp.int32
    )
    before = jnp.cumsum(onehot, axis=0) - onehot
    targets = flat_ids * slot_cap + jnp.sum(before * onehot, axis=1)
    pair_token = jnp.arange(flat_ids.shape[0], dtype=jnp.int32) // routes.shape[1]
    slot_token = jnp.zeros((experts_n * slot_cap,), jnp.int32).at[targets].set(pair_token)
    slot_live = jnp.zeros((experts_n * slot_cap,), jnp.int32).at[targets].set(1)
    return (targets, slot_token, slot_live)


def per_device(
    query_rows,
    key_rows,
    value_rows,
    sink_logits,
    out_weight,
    stream_in,
    norm_gain,
    routes,
    route_weights,
    gate_weight,
    up_weight,
    down_weight,
):
    tok_count = query_rows.shape[0]
    local_heads = query_rows.shape[1] // HEAD_DIM
    tp_index = lax.axis_index(TP)
    kv_group = tp_index * local_heads // REP
    own_keys = lax.dynamic_slice_in_dim(key_rows, kv_group * HEAD_DIM, HEAD_DIM, 1)
    own_values = lax.dynamic_slice_in_dim(value_rows, kv_group * HEAD_DIM, HEAD_DIM, 1)
    prior_keys, prior_values = shifted(
        (own_keys[tok_count - WINDOW :], own_values[tok_count - WINDOW :]), "sp", 1
    )
    key_block = jnp.concatenate([prior_keys, own_keys], axis=0)
    value_block = jnp.concatenate([prior_values, own_values], axis=0)
    offset = lax.axis_index("sp") * tok_count
    query_pos = offset + jnp.arange(tok_count, dtype=jnp.int32)
    key_pos = offset - WINDOW + jnp.arange(tok_count + WINDOW, dtype=jnp.int32)
    distance = query_pos[:, None] - key_pos[None, :]
    allowed = (distance >= 0) & (distance < WINDOW) & (key_pos >= 0)[None, :]
    queries = query_rows.reshape(tok_count, local_heads, HEAD_DIM)
    scores = jnp.einsum(
        "qhd,kd->hqk", queries, key_block, preferred_element_type=jnp.float32
    ) * HEAD_DIM ** (-0.5)
    scores = jnp.where(allowed[None], scores, -1e30)
    sink_col = sink_logits.reshape(local_heads, 1, 1)
    row_peak = jnp.maximum(jnp.max(scores, axis=-1, keepdims=True), sink_col)
    exp_terms = jnp.exp(scores - row_peak)
    denom_sum = jnp.sum(exp_terms, axis=-1, keepdims=True) + jnp.exp(sink_col - row_peak)
    attn_probs = (exp_terms / denom_sum).astype(jnp.bfloat16)
    attended = jnp.einsum(
        "hqk,kd->qhd", attn_probs, value_block, preferred_element_type=jnp.float32
    )
    attended = attended.astype(jnp.bfloat16).reshape(tok_count, local_heads * HEAD_DIM)
    width = out_weight.shape[1]
    width_share = width // lax.axis_size(TP)
    projected = sum_at_owner(
        jnp.dot(attended, out_weight, preferred_element_type=jnp.float32).astype(jnp.bfloat16),
        TP,
        1,
    )
    own_input = lax.dynamic_slice_in_dim(stream_in, tp_index * width_share, width_share, 1)
    columns = (own_input.astype(jnp.float32) + projected).astype(jnp.bfloat16)
    experts_n = lax.axis_size("sp")
    top_count = routes.shape[1]
    slot_cap = 3 * tok_count * top_count // (2 * experts_n)
    targets, slot_token, slot_live = slot_tables(routes, experts_n, slot_cap)
    outgoing = jnp.where(slot_live[:, None] > 0, columns[slot_token], jnp.zeros((), jnp.bfloat16))
    outgoing = outgoing.reshape(experts_n, slot_cap, width_share)
    arrived = lax.all_to_all(outgoing, "sp", split_axis=0, concat_axis=0, tiled=True)
    arrived = rms_scale(gathered_copies(arrived, TP, 2), norm_gain)
    sources = arrived.shape[0]
    item_count = arrived.shape[1]
    flat_rows = arrived.reshape(sources * item_count, arrived.shape[2])
    gate_act = jnp.dot(flat_rows, gate_weight[0], preferred_element_type=jnp.float32)
    up_act = jnp.dot(flat_rows, up_weight[0], preferred_element_type=jnp.float32)
    hidden = (jax.nn.silu(gate_act) * up_act).astype(jnp.bfloat16)
    partial_value = jnp.dot(hidden, down_weight[0], preferred_element_type=jnp.float32).astype(
        jnp.bfloat16
    )
    pieces = exchange_in_pieces(partial_value[None], TP, 1, 2, 0)
    summed = jnp.sum(pieces.astype(jnp.float32), axis=0)
    summed = summed.reshape(sources, item_count, summed.shape[1])
    returned = lax.all_to_all(
        summed.astype(jnp.bfloat16), "sp", split_axis=0, concat_axis=0, tiled=True
    ).astype(summed.dtype)
    returned_flat = returned.reshape(experts_n * slot_cap, returned.shape[2])
    pair_weights = route_weights.reshape(-1)
    chosen = returned_flat[targets] * pair_weights[:, None]
    moe_columns = jnp.sum(chosen.reshape(tok_count, top_count, chosen.shape[1]), axis=1)
    out_columns = (columns.astype(jnp.float32) + moe_columns).astype(jnp.bfloat16)
    return lax.all_to_all(out_columns, TP, split_axis=0, concat_axis=1, tiled=True)


def solution(mesh):
    finer = Mesh(mesh.devices.reshape(mesh.shape["sp"], 4, 4), ("sp", "tp_0", "tp_1"))
    placed = (
        P("sp", TP),
        P("sp", None),
        P("sp", None),
        P(TP),
        P(TP, None),
        P("sp", None),
        P(),
        P("sp", None),
        P("sp", None),
        P("sp", None, TP),
        P("sp", None, TP),
        P("sp", TP, None),
    )
    return jax.shard_map(
        per_device, mesh=finer, in_specs=placed, out_specs=P(SP_TP, None), check_vma=False
    )
```

profile of v0, /device:TPU:2, one launch (start us, length us, event | category | flops | bytes accessed | tf_op | source)
XLA Modules:
  0.0 221.7 jit_solution(14790796120273187725)
XLA Ops:
  0.0 1.0 constant_dynamic-slice_fusion
  1.1 1.7 collective-permute-start.1
  2.9 0.9 constant_dynamic-slice_fusion.1
  3.9 4.2 %collective-permute-start = (bf16[128,64]{0,1:T(8,128)(2,1)S(1)}, bf16[128,64]{0,1:T(8,128)(2,1)S(1)}, u32[]{:S(2)}, u32[]{:S(2)}) collective-permute-start(bf16[128,64]{0,1:T(8,128)(2,1)S(1)} %slice.20), channel_id=1, source_target_pairs={{0,16},{16,32},{32,48},{48,64},{64,80},{80,96},{96,112},{112,128},... | collective-permute-start | bytes 49160 | tf_op jit(solution)/shard_map/ppermute | solution.py:18
  8.2 0.8 copy.35
  9.1 0.7 broadcast_multiply_fusion
  9.7 0.1 eq.29
  9.9 1.2 reduce-window.6
  11.1 0.2 fusion.30
  11.3 0.2 slice_reduce_fusion
  11.5 0.1 eq.25
  11.6 0.9 copy.31
  12.6 0.1 copy.34
  12.7 0.1 mul.101
  12.9 0.3 fusion.49
  13.2 0.7 broadcast_maximum_fusion
  14.2 0.3 convolution_convert_fusion.2
  14.4 0.4 fusion.11
  14.9 1.3 copy.69
  16.2 7.5 %all-to-all-start = ((bf16[16,256,128]{2,1,0:T(8,128)(2,1)}), bf16[16,256,128]{2,1,0:T(8,128)(2,1)S(1)}, u32[]{:S(2)}, u32[]{:S(2)}) async-start(bf16[16,256,128]{2,1,0:T(8,128)(2,1)} %bitcast.94), calls=%async_computation | async-start | bytes 2097152 | tf_op jit(solution)/shard_map/all_to_all | solution.py:28
  23.8 2.4 %scatter_custom_fusion.1 = s32[768]{0:T(1024)S(1)} fusion(s32[512]{0:T(512)S(1)} %bitcast.105, s32[512]{0:T(512)S(1)} %add_select_fusion, s32[]{:T(128)} %constant.30.clone.1), kind=kCustom, calls=%fused_computation.72 | custom fusion | bytes 3076 | tf_op jit(solution)/shard_map/scatter | solution.py:85
  26.2 2.4 %scatter_custom_fusion = s32[768]{0:T(1024)S(1)} fusion(s32[512]{0:T(512)S(1)} %bitcast.106, s32[512]{0:T(512)S(1)} %broadcast.197, s32[]{:T(128)} %constant.30.clone.1), kind=kCustom, calls=%fused_computation.75 | custom fusion | bytes 3076 | tf_op jit(solution)/shard_map/scatter | solution.py:86
  28.8 10.8 %all-to-all-done = bf16[16,256,128]{2,1,0:T(8,128)(2,1)S(1)} async-done(((bf16[16,256,128]{2,1,0:T(8,128)(2,1)}), bf16[16,256,128]{2,1,0:T(8,128)(2,1)S(1)}, u32[]{:S(2)}, u32[]{:S(2)}) %all-to-all-start) | async-done | bytes 1048608 | tf_op jit(solution)/shard_map/all_to_all | solution.py:28
  39.6 0.1 convert_reduce_fusion
  39.7 0.9 add_convert_fusion.1
  40.6 1.9 gather_fusion
  42.5 0.2 broadcast_select_fusion
  42.7 34.4 %all_to_all.44 = bf16[32,24,128]{2,1,0:T(8,128)(2,1)S(1)} all-to-all(bf16[32,24,128]{2,1,0:T(8,128)(2,1)S(1)} %broadcast_select_fusion), channel_id=1, replica_groups=mesh['sp'=32,'tp_0'=4,'tp_1'=4] {'sp'}, dimensions={0} | all-to-all | bytes 393216 | tf_op jit(solution)/shard_map/all_to_all | solution.py:149
  77.1 0.6 broadcast_in_dim.55
  77.7 42.4 %all_to_all.45 = bf16[16,32,24,128]{3,2,1,0:T(8,128)(2,1)S(1)} all-to-all(bf16[16,32,24,128]{3,2,1,0:T(8,128)(2,1)S(1)} %broadcast_in_dim.55), channel_id=1, replica_groups=mesh['sp'=32,'tp_0'=4,'tp_1'=4] {'tp_0','tp_1'}, dimensions={0} | all-to-all | bytes 6291456 | tf_op jit(solution)/shard_map/all_to_all | solution.py:40
  120.1 0.7 fusion
  120.8 1.1 fusion.3
  121.9 3.6 %copy.38 = bf16[32,24,16,128]{3,2,1,0:T(8,128)(2,1)S(1)} copy(bf16[32,24,16,128]{3,1,0,2:T(8,128)(2,1)S(1)} %fusion.3) | data formatting | bytes 6291456 | tf_op jit(solution)/shard_map/convert_element_type | solution.py:74
  125.6 1.7 copy-done.1
  127.2 1.0 fusion.6
  128.2 0.2 copy-done.7
  128.5 6.9 %fusion.10 = bf16[96,8,16,128]{3,1,2,0:T(8,128)(2,1)} fusion(bf16[1,256,2048]{2,1,0:T(8,128)(2,1)S(1)} %copy-done, bf16[96,8,16,128]{3,2,1,0:T(8,128)(2,1)} %bitcast.98, bf16[1,2048,256]{2,1,0:T(8,128)(2,1)S(1)} %copy-done.7, f32[768,256]{1,0:T(8,128)S(1)} %fusion.6), kind=kOutput, calls=%fused_computation.20 | convolution fusion | flops 1613365248 | bytes 9175040 | tf_op jit(solution)/shard_map/dot_general | solution.py:157
  135.4 2.9 %copy.49 = bf16[96,8,16,128]{3,2,1,0:T(8,128)(2,1)S(1)} copy(bf16[96,8,16,128]{3,1,2,0:T(8,128)(2,1)} %fusion.10) | data formatting | bytes 6291456
  138.3 0.8 copy.68
  139.1 43.4 %all_to_all.46 = bf16[16,1,768,128]{3,2,1,0:T(8,128)(2,1)} all-to-all(bf16[16,1,768,128]{3,2,1,0:T(8,128)(2,1)S(1)} %bitcast.96), channel_id=1, replica_groups=mesh['sp'=32,'tp_0'=4,'tp_1'=4] {'tp_0','tp_1'}, dimensions={0} | all-to-all | bytes 6291456 | tf_op jit(solution)/shard_map/all_to_all | solution.py:67
  182.5 3.1 %reduce_sum.64 = bf16[768,128]{1,0:T(8,128)(2,1)} reduce(bf16[16,1,768,128]{3,2,1,0:T(8,128)(2,1)} %all_to_all.46, bf16[]{:T(256)} %constant.87.clone.1), dimensions={0,1}, to_apply=%region_9.10 | reduce | flops 1474560 | bytes 3342338 | tf_op jit(solution)/shard_map/reduce_sum | solution.py:161
  185.5 3.9 %all-to-all-start.4 = ((bf16[32,24,128]{2,1,0:T(8,128)(2,1)}), bf16[32,24,128]{2,1,0:T(8,128)(2,1)S(1)}, u32[]{:S(2)}, u32[]{:S(2)}) async-start(bf16[32,24,128]{2,1,0:T(8,128)(2,1)} %bitcast.17), calls=%async_computation.4 | async-start | bytes 393216 | tf_op jit(solution)/shard_map/all_to_all | solution.py:163
  189.4 0.1 copy.40
  189.6 19.8 %all-to-all-done.4 = bf16[32,24,128]{2,1,0:T(8,128)(2,1)S(1)} async-done(((bf16[32,24,128]{2,1,0:T(8,128)(2,1)}), bf16[32,24,128]{2,1,0:T(8,128)(2,1)S(1)}, u32[]{:S(2)}, u32[]{:S(2)}) %all-to-all-start.4) | async-done | bytes 196640 | tf_op jit(solution)/shard_map/all_to_all | solution.py:163
  209.4 1.0 gather_fusion.1
  210.5 0.4 multiply_reduce_fusion
  210.9 10.2 %all_to_all.47 = bf16[16,16,128]{2,1,0:T(8,128)(2,1)S(1)} all-to-all(bf16[16,16,128]{2,1,0:T(8,128)(2,1)S(1)} %bitcast.101), channel_id=1, replica_groups=mesh['sp'=32,'tp_0'=4,'tp_1'=4] {'tp_0','tp_1'}, dimensions={0} | all-to-all | bytes 131072 | tf_op jit(solution)/shard_map/all_to_all | solution.py:171
  221.1 0.6 copy_bitcast_fusion.1
  (40 shorter events, 0.8 us)
Async XLA Ops:
  0.0 128.2 %copy-start = (bf16[1,256,2048]{2,1,0:T(8,128)(2,1)S(1)}, bf16[1,256,2048]{2,1,0:T(8,128)(2,1)}, u32[]{:S(2)}) copy-start(bf16[1,256,2048]{2,1,0:T(8,128)(2,1)} %param.23) | copy-start | bytes 3145732
  0.0 14.1 %copy-start.5 = (f32[2]{0:T(128)S(1)}, f32[2]{0:T(128)}, u32[]{:S(2)}) copy-start(f32[2]{0:T(128)} %param.15) | copy-start | bytes 28
  1.1 11.8 %collective-permute-start.1 = (bf16[128,64]{0,1:T(8,128)(2,1)S(1)}, bf16[128,64]{0,1:T(8,128)(2,1)S(1)}, u32[]{:S(2)}, u32[]{:S(2)}) collective-permute-start(bf16[128,64]{0,1:T(8,128)(2,1)S(1)} %slice.21), channel_id=1, source_target_pairs={{0,16},{16,32},{32,48},{48,64},{64,80},{80,96},{96,112},{112,128},... | collective-permute-start | bytes 49160 | tf_op jit(solution)/shard_map/ppermute | solution.py:18
  3.9 10.5 %copy-start.2 = (bf16[128,2048]{1,0:T(8,128)(2,1)S(1)}, bf16[128,2048]{1,0:T(8,128)(2,1)}, u32[]{:S(2)}) copy-start(bf16[128,2048]{1,0:T(8,128)(2,1)} %param.16) | copy-start | bytes 1572868
  3.9 10.2 %collective-permute-start = (bf16[128,64]{0,1:T(8,128)(2,1)S(1)}, bf16[128,64]{0,1:T(8,128)(2,1)S(1)}, u32[]{:S(2)}, u32[]{:S(2)}) collective-permute-start(bf16[128,64]{0,1:T(8,128)(2,1)S(1)} %slice.20), channel_id=1, source_target_pairs={{0,16},{16,32},{32,48},{48,64},{64,80},{80,96},{96,112},{112,128},... | collective-permute-start | bytes 49160 | tf_op jit(solution)/shard_map/ppermute | solution.py:18
  16.2 23.4 %all-to-all-start = ((bf16[16,256,128]{2,1,0:T(8,128)(2,1)}), bf16[16,256,128]{2,1,0:T(8,128)(2,1)S(1)}, u32[]{:S(2)}, u32[]{:S(2)}) async-start(bf16[16,256,128]{2,1,0:T(8,128)(2,1)} %bitcast.94), calls=%async_computation | async-start | bytes 2097152 | tf_op jit(solution)/shard_map/all_to_all | solution.py:28
  120.1 0.7 copy-start.3
  121.9 5.3 %copy-start.6 = (bf16[1,2048,256]{2,1,0:T(8,128)(2,1)S(1)}, bf16[1,2048,256]{2,1,0:T(8,128)(2,1)}, u32[]{:S(2)}) copy-start(bf16[1,2048,256]{2,1,0:T(8,128)(2,1)} %param.21) | copy-start | bytes 3145732
  125.6 1.7 copy-start.1
  127.2 1.2 copy-start.7
  182.5 6.9 %copy-start.4 = (f32[256,2]{0,1:T(2,128)S(1)}, f32[256,2]{0,1:T(2,128)}, u32[]{:S(2)}) copy-start(f32[256,2]{0,1:T(2,128)} %param.20) | copy-start | bytes 6148
  185.5 23.8 %all-to-all-start.4 = ((bf16[32,24,128]{2,1,0:T(8,128)(2,1)}), bf16[32,24,128]{2,1,0:T(8,128)(2,1)S(1)}, u32[]{:S(2)}, u32[]{:S(2)}) async-start(bf16[32,24,128]{2,1,0:T(8,128)(2,1)} %bitcast.17), calls=%async_computation.4 | async-start | bytes 393216 | tf_op jit(solution)/shard_map/all_to_all | solution.py:163
where the time goes:
time: 223 us; the launch traced here: 222 us
  blocking collectives  130 us (58%)
  waiting for transfers between devices  30.6 us (14%)
  local copies, waits for them, and re-layouts  24.5 us (11%)
  starting transfers between devices  17.3 us (8%)
  other arithmetic  9.61 us (4%)
  matrix products  8.91 us (4%)
    all_to_all x1, blocking collectives, exchange_in_pieces(): lax.all_to_all(slab, axis, split_axis=0, concat_axis=0, tiled=True)  43.4 us
    all_to_all x1, blocking collectives, sent_to_all(): return lax.all_to_all(copies, axis, split_axis=0, concat_axis=0, tiled=True)  42.4 us
    all_to_all x1, blocking collectives, per_device(): lax.all_to_all(outgoing, 'sp', split_axis=0, concat_axis=0, tiled=True)  34.4 us
    all_to_all x1, waiting for transfers between devices, per_device(): lax.all_to_all(summed.astype(jnp.bfloat16), 'sp', split_axis=0, concat_ax...  19.8 us
    all_to_all x1, waiting for transfers between devices, sum_at_owner(): lax.all_to_all(pieces, axis, split_axis=0, concat_axis=0, tiled=True)  10.8 us
    all_to_all x1, blocking collectives, per_device(): lax.all_to_all(out_columns, TP, split_axis=0, concat_axis=1, tiled=True)  10.2 us
    all_to_all x1, starting transfers between devices, sum_at_owner(): lax.all_to_all(pieces, axis, split_axis=0, concat_axis=0, tiled=True)  7.48 us
    dot_general x1, matrix products, per_device(): jnp.dot(hidden, down_weight[0], preferred_element_type=jnp.float32)  6.92 us
  transfers between devices with their start and end apart: 4, of which 2 were waited for; matrix products, arithmetic and copies ran while one was open for 5% of the time, Pallas kernels for 0%

commit v1 on v0

--- a/solution.py
+++ b/solution.py
@@ -168,7 +168,10 @@
     chosen = returned_flat[targets] * pair_weights[:, None]
     moe_columns = jnp.sum(chosen.reshape(tok_count, top_count, chosen.shape[1]), axis=1)
     out_columns = (columns.astype(jnp.float32) + moe_columns).astype(jnp.bfloat16)
-    return lax.all_to_all(out_columns, TP, split_axis=0, concat_axis=1, tiled=True)
+    return jnp.concatenate(
+        lax.all_to_all(jnp.stack(jnp.split(out_columns, lax.axis_size(TP), axis=0)), TP, 0, 0),
+        axis=1,
+    )
 
 
 def solution(mesh):

time: 223 us -> 223 us (level)
    unnamed x22 -> x37, local copies, waits for them, and re-layouts: 6.88 us -> 7.01 us
where the time goes in v1:
time: 223 us; the launch traced here: 222 us
  blocking collectives  130 us (58%)
  waiting for transfers between devices  30.6 us (14%)
  local copies, waits for them, and re-layouts  24.6 us (11%)
  starting transfers between devices  17.3 us (8%)
  other arithmetic  9.61 us (4%)
  matrix products  8.91 us (4%)
    all_to_all x1, blocking collectives, exchange_in_pieces(): lax.all_to_all(slab, axis, split_axis=0, concat_axis=0, tiled=True)  43.4 us
    all_to_all x1, blocking collectives, sent_to_all(): return lax.all_to_all(copies, axis, split_axis=0, concat_axis=0, tiled=True)  42.4 us
    all_to_all x1, blocking collectives, per_device(): lax.all_to_all(outgoing, 'sp', split_axis=0, concat_axis=0, tiled=True)  34.4 us
    all_to_all x1, waiting for transfers between devices, per_device(): lax.all_to_all(summed.astype(jnp.bfloat16), 'sp', split_axis=0, concat_ax...  19.8 us
    all_to_all x1, waiting for transfers between devices, sum_at_owner(): lax.all_to_all(pieces, axis, split_axis=0, concat_axis=0, tiled=True)  10.8 us
    all_to_all x1, blocking collectives, per_device(): lax.all_to_all(jnp.stack(jnp.split(out_columns, lax.axis_size(TP), axis=0...  10.2 us
    all_to_all x1, starting transfers between devices, sum_at_owner(): lax.all_to_all(pieces, axis, split_axis=0, concat_axis=0, tiled=True)  7.48 us
    unnamed x37, local copies, waits for them, and re-layouts  7.01 us
  transfers between devices with their start and end apart: 4, of which 2 were waited for; matrix products, arithmetic and copies ran while one was open for 5% of the time, Pallas kernels for 0%

profile of v1, /device:TPU:2, one launch (start us, length us, event | category | flops | bytes accessed | tf_op | source)
XLA Modules:
  0.0 221.9 jit_solution(13956166881251069340)
XLA Ops:
  0.0 1.0 constant_dynamic-slice_fusion
  1.1 1.7 collective-permute-start.1
  2.9 0.9 constant_dynamic-slice_fusion.1
  3.9 4.2 %collective-permute-start = (bf16[128,64]{0,1:T(8,128)(2,1)S(1)}, bf16[128,64]{0,1:T(8,128)(2,1)S(1)}, u32[]{:S(2)}, u32[]{:S(2)}) collective-permute-start(bf16[128,64]{0,1:T(8,128)(2,1)S(1)} %slice.20), channel_id=1, source_target_pairs={{0,16},{16,32},{32,48},{48,64},{64,80},{80,96},{96,112},{112,128},... | collective-permute-start | bytes 49160 | tf_op jit(solution)/shard_map/ppermute | solution.py:18
  8.2 0.8 copy.34
  9.1 0.7 broadcast_multiply_fusion
  9.7 0.1 eq.29
  9.9 1.2 reduce-window.6
  11.1 0.2 fusion.30
  11.3 0.2 slice_reduce_fusion
  11.5 0.1 eq.25
  11.6 0.9 copy.30
  12.6 0.1 copy.33
  12.7 0.1 mul.101
  12.9 0.3 fusion.49
  13.2 0.7 broadcast_maximum_fusion
  14.2 0.3 convolution_convert_fusion.2
  14.4 0.4 fusion.11
  14.9 1.3 copy.68
  16.2 7.5 %all-to-all-start = ((bf16[16,256,128]{2,1,0:T(8,128)(2,1)}), bf16[16,256,128]{2,1,0:T(8,128)(2,1)S(1)}, u32[]{:S(2)}, u32[]{:S(2)}) async-start(bf16[16,256,128]{2,1,0:T(8,128)(2,1)} %bitcast.157), calls=%async_computation | async-start | bytes 2097152 | tf_op jit(solution)/shard_map/all_to_all | solution.py:28
  23.8 2.4 %scatter_custom_fusion.1 = s32[768]{0:T(1024)S(1)} fusion(s32[512]{0:T(512)S(1)} %bitcast.167, s32[512]{0:T(512)S(1)} %add_select_fusion, s32[]{:T(128)} %constant.30.clone.1), kind=kCustom, calls=%fused_computation.104 | custom fusion | bytes 3076 | tf_op jit(solution)/shard_map/scatter | solution.py:85
  26.2 2.4 %scatter_custom_fusion = s32[768]{0:T(1024)S(1)} fusion(s32[512]{0:T(512)S(1)} %bitcast.168, s32[512]{0:T(512)S(1)} %broadcast.197, s32[]{:T(128)} %constant.30.clone.1), kind=kCustom, calls=%fused_computation.107 | custom fusion | bytes 3076 | tf_op jit(solution)/shard_map/scatter | solution.py:86
  28.8 10.8 %all-to-all-done = bf16[16,256,128]{2,1,0:T(8,128)(2,1)S(1)} async-done(((bf16[16,256,128]{2,1,0:T(8,128)(2,1)}), bf16[16,256,128]{2,1,0:T(8,128)(2,1)S(1)}, u32[]{:S(2)}, u32[]{:S(2)}) %all-to-all-start) | async-done | bytes 1048608 | tf_op jit(solution)/shard_map/all_to_all | solution.py:28
  39.6 0.1 convert_reduce_fusion
  39.7 0.9 add_convert_fusion.1
  40.6 1.9 gather_fusion
  42.5 0.2 broadcast_select_fusion
  42.7 34.4 %all_to_all.30 = bf16[32,24,128]{2,1,0:T(8,128)(2,1)S(1)} all-to-all(bf16[32,24,128]{2,1,0:T(8,128)(2,1)S(1)} %broadcast_select_fusion), channel_id=1, replica_groups=mesh['sp'=32,'tp_0'=4,'tp_1'=4] {'sp'}, dimensions={0} | all-to-all | bytes 393216 | tf_op jit(solution)/shard_map/all_to_all | solution.py:149
  77.1 0.6 broadcast_in_dim.55
  77.7 42.4 %all_to_all.31 = bf16[16,32,24,128]{3,2,1,0:T(8,128)(2,1)S(1)} all-to-all(bf16[16,32,24,128]{3,2,1,0:T(8,128)(2,1)S(1)} %broadcast_in_dim.55), channel_id=1, replica_groups=mesh['sp'=32,'tp_0'=4,'tp_1'=4] {'tp_0','tp_1'}, dimensions={0} | all-to-all | bytes 6291456 | tf_op jit(solution)/shard_map/all_to_all | solution.py:40
  120.1 0.7 fusion
  120.8 1.1 fusion.3
  121.9 3.6 %copy.37 = bf16[32,24,16,128]{3,2,1,0:T(8,128)(2,1)S(1)} copy(bf16[32,24,16,128]{3,1,0,2:T(8,128)(2,1)S(1)} %fusion.3) | data formatting | bytes 6291456 | tf_op jit(solution)/shard_map/convert_element_type | solution.py:74
  125.6 1.7 copy-done.1
  127.2 1.0 fusion.6
  128.2 0.2 copy-done.7
  128.5 6.9 %fusion.10 = bf16[96,8,16,128]{3,1,2,0:T(8,128)(2,1)} fusion(bf16[1,256,2048]{2,1,0:T(8,128)(2,1)S(1)} %copy-done, bf16[96,8,16,128]{3,2,1,0:T(8,128)(2,1)} %bitcast.161, bf16[1,2048,256]{2,1,0:T(8,128)(2,1)S(1)} %copy-done.7, f32[768,256]{1,0:T(8,128)S(1)} %fusion.6), kind=kOutput, calls=%fused_computation.20 | convolution fusion | flops 1613365248 | bytes 9175040 | tf_op jit(solution)/shard_map/dot_general | solution.py:157
  135.4 2.9 %copy.48 = bf16[96,8,16,128]{3,2,1,0:T(8,128)(2,1)S(1)} copy(bf16[96,8,16,128]{3,1,2,0:T(8,128)(2,1)} %fusion.10) | data formatting | bytes 6291456
  138.3 0.8 copy.67
  139.1 43.4 %all_to_all.32 = bf16[16,1,768,128]{3,2,1,0:T(8,128)(2,1)} all-to-all(bf16[16,1,768,128]{3,2,1,0:T(8,128)(2,1)S(1)} %bitcast.159), channel_id=1, replica_groups=mesh['sp'=32,'tp_0'=4,'tp_1'=4] {'tp_0','tp_1'}, dimensions={0} | all-to-all | bytes 6291456 | tf_op jit(solution)/shard_map/all_to_all | solution.py:67
  182.5 3.1 %reduce_sum.64 = bf16[768,128]{1,0:T(8,128)(2,1)} reduce(bf16[16,1,768,128]{3,2,1,0:T(8,128)(2,1)} %all_to_all.32, bf16[]{:T(256)} %constant.87.clone.1), dimensions={0,1}, to_apply=%region_9.10 | reduce | flops 1474560 | bytes 3342338 | tf_op jit(solution)/shard_map/reduce_sum | solution.py:161
  185.5 3.9 %all-to-all-start.4 = ((bf16[32,24,128]{2,1,0:T(8,128)(2,1)}), bf16[32,24,128]{2,1,0:T(8,128)(2,1)S(1)}, u32[]{:S(2)}, u32[]{:S(2)}) async-start(bf16[32,24,128]{2,1,0:T(8,128)(2,1)} %bitcast.17), calls=%async_computation.4 | async-start | bytes 393216 | tf_op jit(solution)/shard_map/all_to_all | solution.py:163
  189.4 0.1 copy.39
  189.6 19.8 %all-to-all-done.4 = bf16[32,24,128]{2,1,0:T(8,128)(2,1)S(1)} async-done(((bf16[32,24,128]{2,1,0:T(8,128)(2,1)}), bf16[32,24,128]{2,1,0:T(8,128)(2,1)S(1)}, u32[]{:S(2)}, u32[]{:S(2)}) %all-to-all-start.4) | async-done | bytes 196640 | tf_op jit(solution)/shard_map/all_to_all | solution.py:163
  209.4 1.0 gather_fusion.1
  210.5 0.4 multiply_reduce_fusion
  211.1 10.2 %all_to_all.33 = bf16[16,16,128]{2,1,0:T(8,128)(2,1)S(1)} all-to-all(bf16[16,16,128]{2,1,0:T(8,128)(2,1)S(1)} %constant_dynamic-update-slice_fusion), channel_id=1, replica_groups=mesh['sp'=32,'tp_0'=4,'tp_1'=4] {'tp_0','tp_1'}, dimensions={0} | all-to-all | bytes 131072 | tf_op jit(solution)/shard_map/all_to_all | solution.py:172
  221.3 0.6 copy_bitcast_fusion.1
  (56 shorter events, 0.9 us)
Async XLA Ops:
  0.0 128.2 %copy-start = (bf16[1,256,2048]{2,1,0:T(8,128)(2,1)S(1)}, bf16[1,256,2048]{2,1,0:T(8,128)(2,1)}, u32[]{:S(2)}) copy-start(bf16[1,256,2048]{2,1,0:T(8,128)(2,1)} %param.23) | copy-start | bytes 3145732
  0.0 14.1 %copy-start.5 = (f32[2]{0:T(128)S(1)}, f32[2]{0:T(128)}, u32[]{:S(2)}) copy-start(f32[2]{0:T(128)} %param.15) | copy-start | bytes 28
  1.1 11.8 %collective-permute-start.1 = (bf16[128,64]{0,1:T(8,128)(2,1)S(1)}, bf16[128,64]{0,1:T(8,128)(2,1)S(1)}, u32[]{:S(2)}, u32[]{:S(2)}) collective-permute-start(bf16[128,64]{0,1:T(8,128)(2,1)S(1)} %slice.21), channel_id=1, source_target_pairs={{0,16},{16,32},{32,48},{48,64},{64,80},{80,96},{96,112},{112,128},... | collective-permute-start | bytes 49160 | tf_op jit(solution)/shard_map/ppermute | solution.py:18
  3.9 10.5 %copy-start.2 = (bf16[128,2048]{1,0:T(8,128)(2,1)S(1)}, bf16[128,2048]{1,0:T(8,128)(2,1)}, u32[]{:S(2)}) copy-start(bf16[128,2048]{1,0:T(8,128)(2,1)} %param.16) | copy-start | bytes 1572868
  3.9 10.2 %collective-permute-start = (bf16[128,64]{0,1:T(8,128)(2,1)S(1)}, bf16[128,64]{0,1:T(8,128)(2,1)S(1)}, u32[]{:S(2)}, u32[]{:S(2)}) collective-permute-start(bf16[128,64]{0,1:T(8,128)(2,1)S(1)} %slice.20), channel_id=1, source_target_pairs={{0,16},{16,32},{32,48},{48,64},{64,80},{80,96},{96,112},{112,128},... | collective-permute-start | bytes 49160 | tf_op jit(solution)/shard_map/ppermute | solution.py:18
  16.2 23.4 %all-to-all-start = ((bf16[16,256,128]{2,1,0:T(8,128)(2,1)}), bf16[16,256,128]{2,1,0:T(8,128)(2,1)S(1)}, u32[]{:S(2)}, u32[]{:S(2)}) async-start(bf16[16,256,128]{2,1,0:T(8,128)(2,1)} %bitcast.157), calls=%async_computation | async-start | bytes 2097152 | tf_op jit(solution)/shard_map/all_to_all | solution.py:28
  120.1 0.7 copy-start.3
  121.9 5.3 %copy-start.6 = (bf16[1,2048,256]{2,1,0:T(8,128)(2,1)S(1)}, bf16[1,2048,256]{2,1,0:T(8,128)(2,1)}, u32[]{:S(2)}) copy-start(bf16[1,2048,256]{2,1,0:T(8,128)(2,1)} %param.21) | copy-start | bytes 3145732
  125.6 1.7 copy-start.1
  127.2 1.2 copy-start.7
  182.5 6.9 %copy-start.4 = (f32[256,2]{0,1:T(2,128)S(1)}, f32[256,2]{0,1:T(2,128)}, u32[]{:S(2)}) copy-start(f32[256,2]{0,1:T(2,128)} %param.20) | copy-start | bytes 6148
  185.5 23.8 %all-to-all-start.4 = ((bf16[32,24,128]{2,1,0:T(8,128)(2,1)}), bf16[32,24,128]{2,1,0:T(8,128)(2,1)S(1)}, u32[]{:S(2)}, u32[]{:S(2)}) async-start(bf16[32,24,128]{2,1,0:T(8,128)(2,1)} %bitcast.17), calls=%async_computation.4 | async-start | bytes 393216 | tf_op jit(solution)/shard_map/all_to_all | solution.py:163
